TPU v7x, 32 devices: a whole 2x2x4 slice. The times are simulated.
32 devices in a mesh: sp: 8 (over z, y), tp: 4 (over x, core).
Axes of the slice: x: 2, y: 2, z: 4, core: 2. Of those that a mesh axis runs over, the one named last changes fastest.
Arguments:
- hidden: bfloat16 [6144, 2048], P(('sp', 'tp')), may hold values from -6 to 6
- norm_gain: float32 [2, 2048], replicated, may hold values from 0.1 to 1.9
- w_value: bfloat16 [2, 2048, 2048], P(None, 'sp', 'tp'), may hold values from -0.125 to 0.125
- w_gate: bfloat16 [2, 2048, 2048], P(None, 'sp', 'tp'), may hold values from -0.125 to 0.125
- conv_weight: float32 [2, 31, 2048], P(None, None, 'tp'), may hold values from -3 to 3
- conv_bias: float32 [2, 2048], P(None, 'tp'), may hold values from -3 to 3
- chan_gain: float32 [2, 2048], P(None, 'tp'), may hold values from 0.1 to 1.9
- chan_shift: float32 [2, 2048], P(None, 'tp'), may hold values from -3 to 3
- w_out: bfloat16 [2, 2048, 2048], P(None, 'tp', 'sp'), may hold values from -0.125 to 0.125
Outputs:
- result: bfloat16 [6144, 2048], P(('sp', 'tp'))
All inputs are finite; a program needn't handle non-finite values.
Results may differ from a plain program's by a relative error of at most 0.015.
Values may be sent and summed in bfloat16 or wider, within the bound.
A program may use at most 64 MiB of HBM per device.

v0:
```python
import jax
import jax.numpy as jnp
from jax import lax
from jax.sharding import PartitionSpec as P

EPS = 1e-06


def shifted(shard, axis, by):
    size = lax.axis_size(axis)
    pairs = [(i, i + by) for i in range(size) if 0 <= i + by < size]
    return lax.ppermute(shard, axis, pairs)


def body(hidden, norm_gain, w_value, w_gate, conv_weight, conv_bias, chan_gain, chan_shift, w_out):
    group = lax.axis_size("tp")
    own_rows = hidden.shape[0]
    chans = w_value.shape[2]
    taps = conv_weight.shape[1]
    state = hidden
    for layer in range(norm_gain.shape[0]):
        xf = state.astype(jnp.float32)
        scale = lax.rsqrt(jnp.mean(xf * xf, axis=1, keepdims=True) + EPS)
        normed = (xf * scale * norm_gain[layer][None, :]).astype(jnp.bfloat16)
        tokens = lax.all_gather(normed, "tp", axis=0, tiled=True)
        empty = jnp.zeros((tokens.shape[0], chans), jnp.float32)

        def add_both(totals, pieces, start, tokens=tokens):
            return (
                jnp.dot(tokens, pieces[0], preferred_element_type=jnp.float32),
                jnp.dot(tokens, pieces[1], preferred_element_type=jnp.float32),
            )

        lin, gate = add_both(
            (empty, empty),
            (
                lax.all_gather(w_value[layer], "sp", axis=0, tiled=True),
                lax.all_gather(w_gate[layer], "sp", axis=0, tiled=True),
            ),
            jnp.int32(0),
        )
        glu = (lin * jax.nn.sigmoid(gate)).astype(jnp.bfloat16)
        before = shifted(glu[tokens.shape[0] - (taps - 1) :], "sp", 1)
        window = jnp.concatenate([before, glu], axis=0).astype(jnp.float32)
        length = tokens.shape[0]
        mixed = jnp.zeros((length, chans), jnp.float32) + conv_bias[layer][None, :]
        for tap in range(taps):
            mixed = mixed + conv_weight[layer, tap][None, :] * window[tap : tap + length]
        totals = lax.psum((jnp.sum(mixed, axis=1), jnp.sum(mixed * mixed, axis=1)), "tp")
        mean = (totals[0] / (chans * group))[:, None]
        msq = (totals[1] / (chans * group))[:, None]
        var = msq - mean * mean
        act = jax.nn.silu(
            (mixed - mean) * lax.rsqrt(var + EPS) * chan_gain[layer][None, :]
            + chan_shift[layer][None, :]
        ).astype(jnp.bfloat16)

        def project(piece, start, act=act):
            return jnp.dot(act, piece, preferred_element_type=jnp.float32)

        partial_out = project(lax.all_gather(w_out[layer], "sp", axis=1, tiled=True), jnp.int32(0))

        def take_rows(start, count, partial_out=partial_out):
            return partial_out

        update = lax.psum_scatter(
            take_rows(jnp.int32(0), own_rows * lax.axis_size("tp")).astype(jnp.bfloat16),
            "tp",
            scatter_dimension=0,
            tiled=True,
        ).astype(jnp.float32)
        state = (xf + update).astype(jnp.bfloat16)
    return state


def solution(mesh):
    placed = (
        P(("sp", "tp"), None),
        P(),
        P(None, "sp", "tp"),
        P(None, "sp", "tp"),
        P(None, None, "tp"),
        P(None, "tp"),
        P(None, "tp"),
        P(None, "tp"),
        P(None, "tp", "sp"),
    )
    return jax.shard_map(
        body, mesh=mesh, in_specs=placed, out_specs=P(("sp", "tp"), None), check_vma=False
    )
```

profile of v0, /device:TPU:0, one launch (start us, length us, event | category | flops | bytes accessed | tf_op | source)
XLA Modules:
  0.0 466.3 jit_solution(699687578448124518)
XLA Ops:
  6.5 2.0 fusion.101
  12.1 49.2 %all-gather.21.cloned.1.call-done = bf16[1,2048,512]{2,1,0:T(8,128)(2,1)} async-done(((bf16[1,256,512]{2,1,0:T(8,128)(2,1)}), bf16[1,2048,512]{2,1,0:T(8,128)(2,1)}) %all-gather.21.cloned.1.call-update) | async-done | bytes 2097168 | tf_op jit(solution)/shard_map/all_gather | solution.py:38
  61.3 28.6 %all-gather.15.cloned.1.call-done = bf16[768,2048]{1,0:T(8,128)(2,1)} async-done(((bf16[192,2048]{1,0:T(8,128)(2,1)}), bf16[768,2048]{1,0:T(8,128)(2,1)}) %all-gather.15.cloned.1.call-update) | async-done | bytes 3145744 | tf_op jit(solution)/shard_map/all_gather | solution.py:25
  89.9 4.3 fusion.6
  94.3 46.9 %all-gather.19.cloned.1.call-done = bf16[1,2048,512]{2,1,0:T(8,128)(2,1)} async-done(((bf16[1,256,512]{2,1,0:T(8,128)(2,1)}), bf16[1,2048,512]{2,1,0:T(8,128)(2,1)}) %all-gather.19.cloned.1.call-update) | async-done | bytes 2097168 | tf_op jit(solution)/shard_map/all_gather | solution.py:37
  141.2 4.5 multiply_convert_fusion.3
  145.7 2.5 collective-permute-start
  150.0 6.9 %fusion.97 = (f32[768]{0:T(1024)S(1)}, f32[768]{0:T(1024)S(1)}, f32[768,512]{1,0:T(8,128)S(1)}) fusion(f32[798,512]{1,0:T(8,128)S(1)} %maximum_convert_fusion, f32[512]{0:T(512)S(1)} %bitcast.128, f32[512]{0:T(512)S(1)} %bitcast.129, f32[512]{0:T(512)S(1)} %bitcast.130, f32[512]{0:T(512)S(1)} %bitcast.131, f32[512]{0:T(512)S(1)} %bitcast.132, ...), kind=kLoop, calls=%fused_computation.177 | loop fusion | flops 25557504 | bytes 50403328 | tf_op jit(solution)/shard_map/reduce_sum | solution.py:49
  156.9 6.2 %all-reduce.1 = (f32[768]{0:T(1024)S(1)}, f32[768]{0:T(1024)S(1)}) all-reduce(f32[768]{0:T(1024)S(1)} %get-tuple-element.8, f32[768]{0:T(1024)S(1)} %get-tuple-element.7), channel_id=1, replica_groups=mesh['sp'=8,'tp'=4] {'tp'}, use_global_device_ids=true, to_apply=%region_4.0 | all-reduce | flops 1536 | bytes 12288 | tf_op jit(solution)/shard_map/psum | solution.py:49
  163.1 28.9 %all-gather.23.cloned.1.call-done = bf16[1,512,2048]{2,1,0:T(8,128)(2,1)} async-done(((bf16[1,512,256]{2,1,0:T(8,128)(2,1)}), bf16[1,512,2048]{2,1,0:T(8,128)(2,1)}) %all-gather.23.cloned.1.call-update) | async-done | bytes 2097168 | tf_op jit(solution)/shard_map/all_gather | solution.py:61
  192.0 5.3 %convolution_convert_fusion.1 = bf16[768,2048]{1,0:T(8,128)(2,1)} fusion(bf16[1,512,2048]{2,1,0:T(8,128)(2,1)} %all-gather.23.cloned.1.call-done, f32[768,512]{1,0:T(8,128)S(1)} %get-tuple-element.14, f32[512]{0:T(512)S(1)} %bitcast.165, f32[512]{0:T(512)S(1)} %bitcast.164, f32[768]{0:T(1024)S(1)} %get-tuple-element.94, f32[768]{0:T(1024)S(1)} %get-tuple-element.93), kind=kOutput, calls=%fused_computation.1 | convolution fusion | flops 1615724544 | bytes 6825984 | tf_op jit(solution)/shard_map/dot_general | solution.py:59
  198.0 35.6 %reduce-scatter.3.cloned.1.call-done = bf16[192,2048]{1,0:T(8,128)(2,1)} async-done(((bf16[768,2048]{1,0:T(8,128)(2,1)}), bf16[192,2048]{1,0:T(8,128)(2,1)}) %reduce-scatter.3.cloned.1.call-update) | async-done | bytes 786448 | tf_op jit(solution)/shard_map/reduce_scatter | solution.py:66
  237.9 46.8 %all-gather.27.cloned.1.call-done = bf16[1,2048,512]{2,1,0:T(8,128)(2,1)} async-done(((bf16[1,256,512]{2,1,0:T(8,128)(2,1)}), bf16[1,2048,512]{2,1,0:T(8,128)(2,1)}) %all-gather.27.cloned.1.call-update) | async-done | bytes 2097168 | tf_op jit(solution)/shard_map/all_gather | solution.py:38
  284.7 28.6 %all-gather.17.cloned.1.call-done = bf16[768,2048]{1,0:T(8,128)(2,1)} async-done(((bf16[192,2048]{1,0:T(8,128)(2,1)}), bf16[768,2048]{1,0:T(8,128)(2,1)}) %all-gather.17.cloned.1.call-update) | async-done | bytes 3145744 | tf_op jit(solution)/shard_map/all_gather | solution.py:25
  313.3 4.3 fusion.1
  317.6 46.9 %all-gather.25.cloned.1.call-done = bf16[1,2048,512]{2,1,0:T(8,128)(2,1)} async-done(((bf16[1,256,512]{2,1,0:T(8,128)(2,1)}), bf16[1,2048,512]{2,1,0:T(8,128)(2,1)}) %all-gather.25.cloned.1.call-update) | async-done | bytes 2097168 | tf_op jit(solution)/shard_map/all_gather | solution.py:37
  364.5 4.5 multiply_convert_fusion.1
  369.0 2.7 collective-permute-start.1
  373.3 6.9 %fusion.96 = (f32[768]{0:T(1024)S(1)}, f32[768]{0:T(1024)S(1)}, f32[768,512]{1,0:T(8,128)S(1)}) fusion(f32[798,512]{1,0:T(8,128)S(1)} %maximum_convert_fusion.1, f32[512]{0:T(512)S(1)} %bitcast.109, f32[512]{0:T(512)S(1)} %bitcast.98, f32[512]{0:T(512)S(1)} %bitcast.142, f32[512]{0:T(512)S(1)} %bitcast.143, f32[512]{0:T(512)S(1)} %bitcast.144, ...), kind=kLoop, calls=%fused_computation.176 | loop fusion | flops 25557504 | bytes 50403328 | tf_op jit(solution)/shard_map/reduce_sum | solution.py:49
  380.2 6.2 %all-reduce = (f32[768]{0:T(1024)S(1)}, f32[768]{0:T(1024)S(1)}) all-reduce(f32[768]{0:T(1024)S(1)} %get-tuple-element.6, f32[768]{0:T(1024)S(1)} %get-tuple-element.5), channel_id=1, replica_groups=mesh['sp'=8,'tp'=4] {'tp'}, use_global_device_ids=true, to_apply=%region_10.11 | all-reduce | flops 1536 | bytes 12288 | tf_op jit(solution)/shard_map/psum | solution.py:49
  386.4 29.1 %all-gather.29.cloned.1.call-done = bf16[1,512,2048]{2,1,0:T(8,128)(2,1)} async-done(((bf16[1,512,256]{2,1,0:T(8,128)(2,1)}), bf16[1,512,2048]{2,1,0:T(8,128)(2,1)}) %all-gather.29.cloned.1.call-update) | async-done | bytes 2097168 | tf_op jit(solution)/shard_map/all_gather | solution.py:61
  415.5 5.3 %convolution_convert_fusion = bf16[768,2048]{1,0:T(8,128)(2,1)} fusion(bf16[1,512,2048]{2,1,0:T(8,128)(2,1)} %all-gather.29.cloned.1.call-done, f32[768,512]{1,0:T(8,128)S(1)} %get-tuple-element.13, f32[512]{0:T(512)S(1)} %bitcast.163, f32[512]{0:T(512)S(1)} %bitcast.162, f32[768]{0:T(1024)S(1)} %get-tuple-element.86, f32[768]{0:T(1024)S(1)} %get-tuple-element.85), kind=kOutput, calls=%fused_computation | convolution fusion | flops 1615724544 | bytes 6825984 | tf_op jit(solution)/shard_map/dot_general | solution.py:59
  420.9 36.2 %reduce-scatter.5.cloned.1.call-done = bf16[192,2048]{1,0:T(8,128)(2,1)} async-done(((bf16[768,2048]{1,0:T(8,128)(2,1)}), bf16[192,2048]{1,0:T(8,128)(2,1)}) %reduce-scatter.5.cloned.1.call-update) | async-done | bytes 786448 | tf_op jit(solution)/shard_map/reduce_scatter | solution.py:66
  457.1 2.4 fusion.17
  (62 shorter events, 11.8 us)
Async XLA Ops:
  6.5 2.1 copy-start
  6.5 2.3 copy-start.5
  6.5 54.8 %all-gather.21.cloned.1.call-start = ((), (), s32[]{:S(2)}) async-start(), calls=%async_computation.7 | async-start | bytes 2359296 | tf_op jit(solution)/shard_map/all_gather | solution.py:38
  8.5 1.6 copy-start.2
  8.5 81.4 %all-gather.15.cloned.1.call-start = ((), (), s32[]{:S(2)}) async-start(), calls=%async_computation.2 | async-start | bytes 3932160 | tf_op jit(solution)/shard_map/all_gather | solution.py:25
  8.9 2.2 copy-start.3
  10.0 2.0 copy-start.4
  10.0 2.0 copy-start.6
  10.1 2.1 copy-start.7
  10.1 131.1 %all-gather.19.cloned.1.call-start = ((), (), s32[]{:S(2)}) async-start(), calls=%async_computation.6 | async-start | bytes 2359296 | tf_op jit(solution)/shard_map/all_gather | solution.py:37
  11.0 181.0 %all-gather.23.cloned.1.call-start = ((), (), s32[]{:S(2)}) async-start(), calls=%async_computation.8 | async-start | bytes 2359296 | tf_op jit(solution)/shard_map/all_gather | solution.py:61
  11.9 221.6 %reduce-scatter.3.cloned.1.call-start = ((), (), s32[]{:S(2)}) async-start(), calls=%async_computation.3 | async-start | bytes 3932160 | tf_op jit(solution)/shard_map/reduce_scatter | solution.py:66
  94.3 53.9 %copy-start.8 = (f32[2,512]{1,0:T(2,128)S(1)}, f32[2,512]{1,0:T(2,128)}, u32[]{:S(2)}) copy-start(f32[2,512]{1,0:T(2,128)} %param.16) | copy-start | bytes 12292
  145.7 4.0 collective-permute-start
  197.4 87.3 %all-gather.27.cloned.1.call-start = ((), (), s32[]{:S(2)}) async-start(), calls=%async_computation.10 | async-start | bytes 2359296 | tf_op jit(solution)/shard_map/all_gather | solution.py:38
  197.9 115.4 %all-gather.17.cloned.1.call-start = ((), (), s32[]{:S(2)}) async-start(), calls=%async_computation.4 | async-start | bytes 3932160 | tf_op jit(solution)/shard_map/all_gather | solution.py:25
  233.5 1.6 copy-start.1
  236.4 128.2 %all-gather.25.cloned.1.call-start = ((), (), s32[]{:S(2)}) async-start(), calls=%async_computation.9 | async-start | bytes 2359296 | tf_op jit(solution)/shard_map/all_gather | solution.py:37
  237.1 178.4 %all-gather.29.cloned.1.call-start = ((), (), s32[]{:S(2)}) async-start(), calls=%async_computation.11 | async-start | bytes 2359296 | tf_op jit(solution)/shard_map/all_gather | solution.py:61
  237.8 219.2 %reduce-scatter.5.cloned.1.call-start = ((), (), s32[]{:S(2)}) async-start(), calls=%async_computation.5 | async-start | bytes 3932160 | tf_op jit(solution)/shard_map/reduce_scatter | solution.py:66
  369.0 4.1 collective-permute-start.1
Sparse Core Ops, SparseCore 0:
  9.5 51.7 all-gather.20
  62.9 27.0 all-gather.14
  92.1 49.0 all-gather.18
  143.1 48.8 all-gather.22
  197.5 36.0 reduce-scatter.2
  235.5 49.0 all-gather.26
  286.2 27.0 all-gather.16
  315.4 49.0 all-gather.24
  366.6 48.8 all-gather.28
  421.0 36.0 reduce-scatter.4
where the time goes:
time: 467 us; the launch traced here: 466 us
  waiting for transfers between devices  382 us (82%)
  matrix products  28.3 us (6%)
  other arithmetic  20.8 us (4%)
  between operations  13.8 us (3%)
  blocking collectives  12.3 us (3%)
  starting transfers between devices  5.48 us (1%)
    all_gather x2, waiting for transfers between devices, body(): lax.all_gather(w_gate[layer], 'sp', axis=0, tiled=True)  95.9 us
    all_gather x2, waiting for transfers between devices, body(): lax.all_gather(w_value[layer], 'sp', axis=0, tiled=True)  93.8 us
    reduce_scatter x2, waiting for transfers between devices, body(): lax.psum_scatter(take_rows(jnp.int32(0), own_rows * lax.axis_size('tp'))....  71.8 us
    all_gather x2, waiting for transfers between devices, body(): lax.all_gather(w_out[layer], 'sp', axis=1, tiled=True)  58 us
    all_gather x2, waiting for transfers between devices, body(): tokens = lax.all_gather(normed, 'tp', axis=0, tiled=True)  57.3 us
    reduce_sum x2, other arithmetic, body(): jnp.sum(mixed, axis=1)  13.8 us
    psum x2, blocking collectives, body(): lax.psum((jnp.sum(mixed, axis=1), jnp.sum(mixed * mixed, axis=1)), 'tp')  12.3 us
    dot_general x2, matrix products, project(): return jnp.dot(act, piece, preferred_element_type=jnp.float32)  10.7 us
  transfers between devices with their start and end apart: 12, of which 12 were waited for; matrix products, arithmetic and copies ran while one was open for 8% of the time, Pallas kernels for 0%

commit v1 on v0

--- a/solution.py
+++ b/solution.py
@@ -4,6 +4,16 @@
 from jax.sharding import PartitionSpec as P
 
 EPS = 1e-06
+
+
+def around_the_ring(block, name, dim):
+    size = lax.axis_size(name)
+    held, shards = (block, [block])
+    for _ in range(size - 1):
+        held = lax.ppermute(held, name, [(i, (i + 1) % size) for i in range(size)])
+        shards.insert(0, held)
+    line = jnp.concatenate(shards, axis=dim)
+    return jnp.roll(line, (lax.axis_index(name) + 1) * block.shape[dim], axis=dim)
 
 
 def shifted(shard, axis, by):
@@ -22,7 +32,7 @@
         xf = state.astype(jnp.float32)
         scale = lax.rsqrt(jnp.mean(xf * xf, axis=1, keepdims=True) + EPS)
         normed = (xf * scale * norm_gain[layer][None, :]).astype(jnp.bfloat16)
-        tokens = lax.all_gather(normed, "tp", axis=0, tiled=True)
+        tokens = around_the_ring(normed, "tp", 0)
         empty = jnp.zeros((tokens.shape[0], chans), jnp.float32)
 
         def add_both(totals, pieces, start, tokens=tokens):

time: 467 us -> 406 us (0.87)
  waiting for transfers between devices: 382 us -> 291 us
  other arithmetic: 20.8 us -> 49.8 us
    all_gather x2, waiting for transfers between devices: 95.9 us -> 0.34 us  [body(): lax.all_gather(w_gate[layer], 'sp', axis=0, tiled=True)]
    ppermute x0 -> x6, waiting for transfers between devices: none -> 67 us  [around_the_ring(): held = lax.ppermute(held, name, [(i, (i + 1) % size) for i in range(size)])]
    all_gather x2 -> x0, waiting for transfers between devices: 57.3 us -> none  [body(): tokens = lax.all_gather(normed, 'tp', axis=0, tiled=True)]
    concatenate x0 -> x2, other arithmetic: none -> 30.7 us  [around_the_ring(): jnp.roll(line, (lax.axis_index(name) + 1) * block.shape[dim], axis=dim)]
  transfers between devices with their start and end apart: 12 -> 16, of which waited for: 12 -> 15; matrix products, arithmetic and copies ran while one was open for 8% -> 17% of each run, Pallas kernels for 0% -> 0%
where the time goes in v1:
time: 406 us
  waiting for transfers between devices  291 us (72%)
  other arithmetic  49.8 us (12%)
  matrix products  28.2 us (7%)
  between operations  13.8 us (3%)
  blocking collectives  12.3 us (3%)
  starting transfers between devices  6 us (1%)
  local copies, waits for them, and re-layouts  4.86 us (1%)
    all_gather x2, waiting for transfers between devices, body(): lax.all_gather(w_value[layer], 'sp', axis=0, tiled=True)  90.3 us
    reduce_scatter x2, waiting for transfers between devices, body(): lax.psum_scatter(take_rows(jnp.int32(0), own_rows * lax.axis_size('tp'))....  71.2 us
    ppermute x6, waiting for transfers between devices, around_the_ring(): held = lax.ppermute(held, name, [(i, (i + 1) % size) for i in range(size)])  67 us
    all_gather x2, waiting for transfers between devices, body(): lax.all_gather(w_out[layer], 'sp', axis=1, tiled=True)  58.1 us
    concatenate x2, other arithmetic, around_the_ring(): jnp.roll(line, (lax.axis_index(name) + 1) * block.shape[dim], axis=dim)  30.7 us
    reduce_sum x2, other arithmetic, body(): jnp.sum(mixed, axis=1)  13.8 us
    psum x2, blocking collectives, body(): lax.psum((jnp.sum(mixed, axis=1), jnp.sum(mixed * mixed, axis=1)), 'tp')  12.3 us
    dot_general x2, matrix products, project(): return jnp.dot(act, piece, preferred_element_type=jnp.float32)  10.6 us
  transfers between devices with their start and end apart: 16, of which 15 were waited for; matrix products, arithmetic and copies ran while one was open for 17% of the time, Pallas kernels for 0%

profile of v1, /device:TPU:0, one launch (start us, length us, event | category | flops | bytes accessed | tf_op | source)
XLA Modules:
  0.0 406.1 jit_solution(9651381716040389489)
XLA Ops:
  10.6 11.6 %collective-permute-done = bf16[192,2048]{1,0:T(8,128)(2,1)S(1)} collective-permute-done((bf16[192,2048]{1,0:T(8,128)(2,1)S(1)}, bf16[192,2048]{1,0:T(8,128)(2,1)S(1)}, u32[]{:S(2)}, u32[]{:S(2)}) %collective-permute-start) | collective-permute-done | bytes 786464 | tf_op jit(solution)/shard_map/ppermute | solution.py:13
  24.1 9.5 %collective-permute-done.1 = bf16[192,2048]{1,0:T(8,128)(2,1)S(1)} collective-permute-done((bf16[192,2048]{1,0:T(8,128)(2,1)S(1)}, bf16[192,2048]{1,0:T(8,128)(2,1)S(1)}, u32[]{:S(2)}, u32[]{:S(2)}) %collective-permute-start.1) | collective-permute-done | bytes 786464 | tf_op jit(solution)/shard_map/ppermute | solution.py:13
  33.8 11.4 %collective-permute-done.2 = bf16[192,2048]{1,0:T(8,128)(2,1)} collective-permute-done((bf16[192,2048]{1,0:T(8,128)(2,1)S(1)}, bf16[192,2048]{1,0:T(8,128)(2,1)}, u32[]{:S(2)}, u32[]{:S(2)}) %collective-permute-start.2) | collective-permute-done | bytes 786464 | tf_op jit(solution)/shard_map/ppermute | solution.py:13
  45.1 15.8 %fusion.10 = bf16[768,2048]{1,0:T(8,128)(2,1)} fusion(s32[]{:T(128)S(6)} %select_n.13, bf16[192,2048]{1,0:T(8,128)(2,1)} %collective-permute-done.2, bf16[192,2048]{1,0:T(8,128)(2,1)S(1)} %collective-permute-done.1, bf16[192,2048]{1,0:T(8,128)(2,1)S(1)} %collective-permute-done, bf16[192,2048]{1,0:T(8,128)(2,1)S(1)} %fusion.26), kind=kLoop, calls=%fused_computation.28 | loop fusion | flops 25165824 | bytes 6291460 | tf_op jit(solution)/shard_map/jit(_roll_dynamic)/concatenate | solution.py:16
  61.3 4.3 %fusion.20 = f32[768,512]{1,0:T(8,128)S(1)} fusion(bf16[768,2048]{1,0:T(8,128)(2,1)} %fusion.10, bf16[1,2048,512]{2,1,0:T(8,128)(2,1)} %all-gather.15.cloned.1.call-done), kind=kOutput, calls=%fused_computation.44 | convolution fusion | flops 1610612736 | bytes 6815744 | tf_op jit(solution)/shard_map/dot_general | solution.py:41
  65.6 45.4 %all-gather.13.cloned.1.call-done = bf16[1,2048,512]{2,1,0:T(8,128)(2,1)} async-done(((bf16[1,256,512]{2,1,0:T(8,128)(2,1)}), bf16[1,2048,512]{2,1,0:T(8,128)(2,1)}) %all-gather.13.cloned.1.call-update) | async-done | bytes 2097168 | tf_op jit(solution)/shard_map/all_gather | solution.py:47
  111.1 4.5 %multiply_convert_fusion.3 = bf16[768,512]{1,0:T(8,128)(2,1)S(1)} fusion(f32[768,512]{1,0:T(8,128)S(1)} %fusion.20, bf16[768,2048]{1,0:T(8,128)(2,1)} %fusion.10, bf16[1,2048,512]{2,1,0:T(8,128)(2,1)} %all-gather.13.cloned.1.call-done), kind=kOutput, calls=%fused_computation.185 | convolution fusion | flops 1612578816 | bytes 7602176 | tf_op jit(solution)/shard_map/dot_general | solution.py:40
  119.9 6.9 %fusion.111 = (f32[768]{0:T(1024)S(1)}, f32[768]{0:T(1024)S(1)}, f32[768,512]{1,0:T(8,128)S(1)}) fusion(f32[798,512]{1,0:T(8,128)S(1)} %maximum_convert_fusion, f32[512]{0:T(512)S(1)} %bitcast.132, f32[512]{0:T(512)S(1)} %bitcast.133, f32[512]{0:T(512)S(1)} %bitcast.134, f32[512]{0:T(512)S(1)} %bitcast.135, f32[512]{0:T(512)S(1)} %bitcast.136, ...), kind=kLoop, calls=%fused_computation.207 | loop fusion | flops 25557504 | bytes 50403328 | tf_op jit(solution)/shard_map/reduce_sum | solution.py:59
  126.8 6.2 %all-reduce.1 = (f32[768]{0:T(1024)S(1)}, f32[768]{0:T(1024)S(1)}) all-reduce(f32[768]{0:T(1024)S(1)} %get-tuple-element.9, f32[768]{0:T(1024)S(1)} %get-tuple-element.8), channel_id=1, replica_groups=mesh['sp'=8,'tp'=4] {'tp'}, use_global_device_ids=true, to_apply=%region_4.6 | all-reduce | flops 1536 | bytes 12288 | tf_op jit(solution)/shard_map/psum | solution.py:59
  133.0 29.1 %all-gather.17.cloned.1.call-done = bf16[1,512,2048]{2,1,0:T(8,128)(2,1)} async-done(((bf16[1,512,256]{2,1,0:T(8,128)(2,1)}), bf16[1,512,2048]{2,1,0:T(8,128)(2,1)}) %all-gather.17.cloned.1.call-update) | async-done | bytes 2097168 | tf_op jit(solution)/shard_map/all_gather | solution.py:71
  162.0 5.3 %convolution_convert_fusion.1 = bf16[768,2048]{1,0:T(8,128)(2,1)} fusion(bf16[1,512,2048]{2,1,0:T(8,128)(2,1)} %all-gather.17.cloned.1.call-done, f32[768,512]{1,0:T(8,128)S(1)} %get-tuple-element.15, f32[512]{0:T(512)S(1)} %bitcast.165, f32[512]{0:T(512)S(1)} %bitcast.164, f32[768]{0:T(1024)S(1)} %get-tuple-element.95, f32[768]{0:T(1024)S(1)} %get-tuple-element.94), kind=kOutput, calls=%fused_computation.17 | convolution fusion | flops 1615724544 | bytes 6825984 | tf_op jit(solution)/shard_map/dot_general | solution.py:69
  168.6 35.0 %reduce-scatter.3.cloned.1.call-done = bf16[192,2048]{1,0:T(8,128)(2,1)} async-done(((bf16[768,2048]{1,0:T(8,128)(2,1)}), bf16[192,2048]{1,0:T(8,128)(2,1)}) %reduce-scatter.3.cloned.1.call-update) | async-done | bytes 786448 | tf_op jit(solution)/shard_map/reduce_scatter | solution.py:76
  205.6 11.4 %collective-permute-done.4 = bf16[192,2048]{1,0:T(8,128)(2,1)S(1)} collective-permute-done((bf16[192,2048]{1,0:T(8,128)(2,1)S(1)}, bf16[192,2048]{1,0:T(8,128)(2,1)S(1)}, u32[]{:S(2)}, u32[]{:S(2)}) %collective-permute-start.4) | collective-permute-done | bytes 786464 | tf_op jit(solution)/shard_map/ppermute | solution.py:13
  217.0 11.5 %collective-permute-done.5 = bf16[192,2048]{1,0:T(8,128)(2,1)} collective-permute-done((bf16[192,2048]{1,0:T(8,128)(2,1)S(1)}, bf16[192,2048]{1,0:T(8,128)(2,1)}, u32[]{:S(2)}, u32[]{:S(2)}) %collective-permute-start.5) | collective-permute-done | bytes 786464 | tf_op jit(solution)/shard_map/ppermute | solution.py:13
  228.6 11.7 %collective-permute-done.6 = bf16[192,2048]{1,0:T(8,128)(2,1)} collective-permute-done((bf16[192,2048]{1,0:T(8,128)(2,1)}, bf16[192,2048]{1,0:T(8,128)(2,1)}, u32[]{:S(2)}, u32[]{:S(2)}) %collective-permute-start.6) | collective-permute-done | bytes 786464 | tf_op jit(solution)/shard_map/ppermute | solution.py:13
  240.2 14.9 %fusion.3 = bf16[768,2048]{1,0:T(8,128)(2,1)} fusion(s32[]{:T(128)S(6)} %select_n.13, bf16[192,2048]{1,0:T(8,128)(2,1)} %collective-permute-done.6, bf16[192,2048]{1,0:T(8,128)(2,1)} %collective-permute-done.5, bf16[192,2048]{1,0:T(8,128)(2,1)S(1)} %collective-permute-done.4, bf16[192,2048]{1,0:T(8,128)(2,1)S(1)} %fusion.30), kind=kLoop, calls=%fused_computation.21 | loop fusion | flops 25165824 | bytes 6291460 | tf_op jit(solution)/shard_map/jit(_roll_dynamic)/concatenate | solution.py:16
  255.1 4.3 %fusion.15 = f32[768,512]{1,0:T(8,128)S(1)} fusion(bf16[768,2048]{1,0:T(8,128)(2,1)} %fusion.3, bf16[1,2048,512]{2,1,0:T(8,128)(2,1)} %all-gather.21.cloned.1.call-done), kind=kOutput, calls=%fused_computation.39 | convolution fusion | flops 1610612736 | bytes 6815744 | tf_op jit(solution)/shard_map/dot_general | solution.py:41
  259.5 44.9 %all-gather.19.cloned.1.call-done = bf16[1,2048,512]{2,1,0:T(8,128)(2,1)} async-done(((bf16[1,256,512]{2,1,0:T(8,128)(2,1)}), bf16[1,2048,512]{2,1,0:T(8,128)(2,1)}) %all-gather.19.cloned.1.call-update) | async-done | bytes 2097168 | tf_op jit(solution)/shard_map/all_gather | solution.py:47
  304.4 4.5 %multiply_convert_fusion.1 = bf16[768,512]{1,0:T(8,128)(2,1)S(1)} fusion(f32[768,512]{1,0:T(8,128)S(1)} %fusion.15, bf16[768,2048]{1,0:T(8,128)(2,1)} %fusion.3, bf16[1,2048,512]{2,1,0:T(8,128)(2,1)} %all-gather.19.cloned.1.call-done), kind=kOutput, calls=%fused_computation.182 | convolution fusion | flops 1612578816 | bytes 7602176 | tf_op jit(solution)/shard_map/dot_general | solution.py:40
  313.1 6.9 %fusion.110 = (f32[768]{0:T(1024)S(1)}, f32[768]{0:T(1024)S(1)}, f32[768,512]{1,0:T(8,128)S(1)}) fusion(f32[798,512]{1,0:T(8,128)S(1)} %maximum_convert_fusion.1, f32[512]{0:T(512)S(1)} %bitcast.98, f32[512]{0:T(512)S(1)} %bitcast.99, f32[512]{0:T(512)S(1)} %bitcast.142, f32[512]{0:T(512)S(1)} %bitcast.143, f32[512]{0:T(512)S(1)} %bitcast.144, ...), kind=kLoop, calls=%fused_computation.206 | loop fusion | flops 25557504 | bytes 50403328 | tf_op jit(solution)/shard_map/reduce_sum | solution.py:59
  320.0 6.2 %all-reduce = (f32[768]{0:T(1024)S(1)}, f32[768]{0:T(1024)S(1)}) all-reduce(f32[768]{0:T(1024)S(1)} %get-tuple-element.7, f32[768]{0:T(1024)S(1)} %get-tuple-element.6), channel_id=1, replica_groups=mesh['sp'=8,'tp'=4] {'tp'}, use_global_device_ids=true, to_apply=%region_10.12 | all-reduce | flops 1536 | bytes 12288 | tf_op jit(solution)/shard_map/psum | solution.py:59
  326.2 29.1 %all-gather.23.cloned.1.call-done = bf16[1,512,2048]{2,1,0:T(8,128)(2,1)} async-done(((bf16[1,512,256]{2,1,0:T(8,128)(2,1)}), bf16[1,512,2048]{2,1,0:T(8,128)(2,1)}) %all-gather.23.cloned.1.call-update) | async-done | bytes 2097168 | tf_op jit(solution)/shard_map/all_gather | solution.py:71
  355.3 5.3 %convolution_convert_fusion = bf16[768,2048]{1,0:T(8,128)(2,1)} fusion(bf16[1,512,2048]{2,1,0:T(8,128)(2,1)} %all-gather.23.cloned.1.call-done, f32[768,512]{1,0:T(8,128)S(1)} %get-tuple-element.14, f32[512]{0:T(512)S(1)} %bitcast.163, f32[512]{0:T(512)S(1)} %bitcast.162, f32[768]{0:T(1024)S(1)} %get-tuple-element.87, f32[768]{0:T(1024)S(1)} %get-tuple-element.86), kind=kOutput, calls=%fused_computation.16 | convolution fusion | flops 1615724544 | bytes 6825984 | tf_op jit(solution)/shard_map/dot_general | solution.py:69
  360.6 36.2 %reduce-scatter.5.cloned.1.call-done = bf16[192,2048]{1,0:T(8,128)(2,1)} async-done(((bf16[768,2048]{1,0:T(8,128)(2,1)}), bf16[192,2048]{1,0:T(8,128)(2,1)}) %reduce-scatter.5.cloned.1.call-update) | async-done | bytes 786448 | tf_op jit(solution)/shard_map/reduce_scatter | solution.py:76
  (68 shorter events, 20.5 us)
Async XLA Ops:
  6.5 2.0 copy-start.2
  6.5 3.0 copy-start
  6.5 3.2 copy-start.4
  6.5 54.8 %all-gather.15.cloned.1.call-start = ((), (), s32[]{:S(2)}) async-start(), calls=%async_computation.5 | async-start | bytes 2359296 | tf_op jit(solution)/shard_map/all_gather | solution.py:48
  8.5 102.6 %all-gather.13.cloned.1.call-start = ((), (), s32[]{:S(2)}) async-start(), calls=%async_computation.4 | async-start | bytes 2359296 | tf_op jit(solution)/shard_map/all_gather | solution.py:47
  9.4 152.6 %all-gather.17.cloned.1.call-start = ((), (), s32[]{:S(2)}) async-start(), calls=%async_computation.6 | async-start | bytes 2359296 | tf_op jit(solution)/shard_map/all_gather | solution.py:71
  9.7 14.4 %copy-start.5 = (f32[2,512]{1,0:T(2,128)S(1)}, f32[2,512]{1,0:T(2,128)}, u32[]{:S(2)}) copy-start(f32[2,512]{1,0:T(2,128)} %param.16) | copy-start | bytes 12292
  9.7 23.9 %copy-start.6 = (f32[2,512]{1,0:T(2,128)S(1)}, f32[2,512]{1,0:T(2,128)}, u32[]{:S(2)}) copy-start(f32[2,512]{1,0:T(2,128)} %param.17) | copy-start | bytes 12292
  9.8 23.9 %copy-start.3 = (f32[2,31,512]{2,0,1:T(2,128)S(1)}, f32[2,31,512]{2,0,1:T(2,128)}, u32[]{:S(2)}) copy-start(f32[2,31,512]{2,0,1:T(2,128)} %param.15) | copy-start | bytes 380932
  10.1 12.1 %collective-permute-start = (bf16[192,2048]{1,0:T(8,128)(2,1)S(1)}, bf16[192,2048]{1,0:T(8,128)(2,1)S(1)}, u32[]{:S(2)}, u32[]{:S(2)}) collective-permute-start(bf16[192,2048]{1,0:T(8,128)(2,1)S(1)} %fusion.26), channel_id=1, source_target_pairs={{0,1},{1,2},{2,3},{3,0},{4,5},{5,6},{6,7},{7,4},{8,9},{9,10},{10,1... | collective-permute-start | bytes 2359304 | tf_op jit(solution)/shard_map/ppermute | solution.py:13
  22.2 11.4 %collective-permute-start.1 = (bf16[192,2048]{1,0:T(8,128)(2,1)S(1)}, bf16[192,2048]{1,0:T(8,128)(2,1)S(1)}, u32[]{:S(2)}, u32[]{:S(2)}) collective-permute-start(bf16[192,2048]{1,0:T(8,128)(2,1)S(1)} %collective-permute-done), channel_id=1, source_target_pairs={{0,1},{1,2},{2,3},{3,0},{4,5},{5,6},{6,7},{7,4},{8,9},{9,10},{10,1... | collective-permute-start | bytes 2359304 | tf_op jit(solution)/shard_map/ppermute | solution.py:13
  24.1 179.5 %reduce-scatter.3.cloned.1.call-start = ((), (), s32[]{:S(2)}) async-start(), calls=%async_computation.2 | async-start | bytes 3932160 | tf_op jit(solution)/shard_map/reduce_scatter | solution.py:76
  33.6 11.5 %collective-permute-start.2 = (bf16[192,2048]{1,0:T(8,128)(2,1)S(1)}, bf16[192,2048]{1,0:T(8,128)(2,1)}, u32[]{:S(2)}, u32[]{:S(2)}) collective-permute-start(bf16[192,2048]{1,0:T(8,128)(2,1)S(1)} %collective-permute-done.1), channel_id=1, source_target_pairs={{0,1},{1,2},{2,3},{3,0},{4,5},{5,6},{6,7},{7,4},{8,9},{9,10},{10,1... | collective-permute-start | bytes 2359304 | tf_op jit(solution)/shard_map/ppermute | solution.py:13
  65.6 52.6 %copy-start.7 = (f32[2,512]{1,0:T(2,128)S(1)}, f32[2,512]{1,0:T(2,128)}, u32[]{:S(2)}) copy-start(f32[2,512]{1,0:T(2,128)} %param.18) | copy-start | bytes 12292
  115.6 4.1 collective-permute-start.3
  167.4 87.7 %all-gather.21.cloned.1.call-start = ((), (), s32[]{:S(2)}) async-start(), calls=%async_computation.8 | async-start | bytes 2359296 | tf_op jit(solution)/shard_map/all_gather | solution.py:48
  168.0 136.4 %all-gather.19.cloned.1.call-start = ((), (), s32[]{:S(2)}) async-start(), calls=%async_computation.7 | async-start | bytes 2359296 | tf_op jit(solution)/shard_map/all_gather | solution.py:47
  168.6 186.7 %all-gather.23.cloned.1.call-start = ((), (), s32[]{:S(2)}) async-start(), calls=%async_computation.9 | async-start | bytes 2359296 | tf_op jit(solution)/shard_map/all_gather | solution.py:71
  203.6 1.6 copy-start.1
  205.5 11.5 %collective-permute-start.4 = (bf16[192,2048]{1,0:T(8,128)(2,1)S(1)}, bf16[192,2048]{1,0:T(8,128)(2,1)S(1)}, u32[]{:S(2)}, u32[]{:S(2)}) collective-permute-start(bf16[192,2048]{1,0:T(8,128)(2,1)S(1)} %fusion.30), channel_id=1, source_target_pairs={{0,1},{1,2},{2,3},{3,0},{4,5},{5,6},{6,7},{7,4},{8,9},{9,10},{10,1... | collective-permute-start | bytes 2359304 | tf_op jit(solution)/shard_map/ppermute | solution.py:13
  217.0 11.5 %collective-permute-start.5 = (bf16[192,2048]{1,0:T(8,128)(2,1)S(1)}, bf16[192,2048]{1,0:T(8,128)(2,1)}, u32[]{:S(2)}, u32[]{:S(2)}) collective-permute-start(bf16[192,2048]{1,0:T(8,128)(2,1)S(1)} %collective-permute-done.4), channel_id=1, source_target_pairs={{0,1},{1,2},{2,3},{3,0},{4,5},{5,6},{6,7},{7,4},{8,9},{9,10},{10,1... | collective-permute-start | bytes 2359304 | tf_op jit(solution)/shard_map/ppermute | solution.py:13
  228.5 11.7 %collective-permute-start.6 = (bf16[192,2048]{1,0:T(8,128)(2,1)}, bf16[192,2048]{1,0:T(8,128)(2,1)}, u32[]{:S(2)}, u32[]{:S(2)}) collective-permute-start(bf16[192,2048]{1,0:T(8,128)(2,1)} %collective-permute-done.5), channel_id=1, source_target_pairs={{0,1},{1,2},{2,3},{3,0},{4,5},{5,6},{6,7},{7,4},{8,9},{9,10},{10,1... | collective-permute-start | bytes 2359304 | tf_op jit(solution)/shard_map/ppermute | solution.py:13
  228.5 168.3 %reduce-scatter.5.cloned.1.call-start = ((), (), s32[]{:S(2)}) async-start(), calls=%async_computation.3 | async-start | bytes 3932160 | tf_op jit(solution)/shard_map/reduce_scatter | solution.py:76
  308.8 4.0 collective-permute-start.7
Sparse Core Ops, SparseCore 0:
  9.5 51.7 all-gather.14
  63.4 47.6 all-gather.12
  113.1 48.8 all-gather.16
  167.5 36.0 reduce-scatter.2
  205.6 49.0 all-gather.20
  256.7 47.6 all-gather.18
  306.4 48.8 all-gather.22
  360.8 36.0 reduce-scatter.4
